TPU v7x, 128 devices: a whole 4x4x4 slice. The times are simulated.
128 devices in a mesh: sp: 32 (over z, y, core), tp: 4 (over x).
Axes of the slice: x: 4, y: 4, z: 4, core: 2. Of those that a mesh axis runs over, the one named last changes fastest.
Arguments:
- residual_entry_input: bfloat16 [32768, 2048], P(('sp', 'tp')), may hold values from -6 to 6
- query_matrix_rows: bfloat16 [32768, 1024], P('sp', 'tp'), may hold values from -6 to 6
- key_matrix_rows: bfloat16 [32768, 1024], P('sp', 'tp'), may hold values from -6 to 6
- value_matrix_rows: bfloat16 [32768, 2048], P('sp', 'tp'), may hold values from -6 to 6
- output_gate_logits: bfloat16 [32768, 2048], P('sp', 'tp'), may hold values from -6 to 6
- input_gate_logits: float32 [32768, 8], P('sp', 'tp'), may hold values from -6 to 6
- forget_gate_logits: float32 [32768, 8], P('sp', 'tp'), may hold values from -8 to 31
- forget_decay_offset: float32 [32768, 8], P('sp', 'tp'), may hold values from -0.7 to 0
- head_norm_gain: float32 [8, 256], P('tp'), may hold values from 0.1 to 1.9
- cell_output_weight: bfloat16 [2048, 2048], P('tp'), may hold values from -0.125 to 0.125
- feedforward_norm_gain: float32 [2048], replicated, may hold values from 0.1 to 1.9
- gate_up_weight: bfloat16 [2048, 5632], P('sp', 'tp'), may hold values from -0.125 to 0.125
- value_up_weight: bfloat16 [2048, 5632], P('sp', 'tp'), may hold values from -0.125 to 0.125
- gate_filter_taps: float32 [3, 5632], P(None, 'tp'), may hold values from -3 to 3
- value_filter_taps: float32 [3, 5632], P(None, 'tp'), may hold values from -3 to 3
- down_projection_weight: bfloat16 [5632, 2048], P('tp', 'sp'), may hold values from -0.078125 to 0.078125
Outputs:
- result: bfloat16 [32768, 2048], P(('sp', 'tp'))
All inputs are finite; a program needn't handle non-finite values.
Results may differ from a plain program's by a relative error of at most 0.025.
Values may be sent and summed in bfloat16 or wider, within the bound.
A program may use at most 128 MiB of HBM per device.

v0:
```python
import jax
import jax.numpy as jnp
from jax import lax
from jax.sharding import Mesh
from jax.sharding import PartitionSpec as P

BLOCK = 128
SP = ("sp_0", "sp_1", "sp_2")
SP_TP = ("sp_0", "sp_1", "sp_2", "tp")
eps = 1e-06
neg_large = -1e30


def neutral_like(x, identity):
    return jax.tree.map(
        lambda part, zero: jnp.zeros_like(part) + jnp.asarray(zero, part.dtype), x, identity
    )


def gathered_once(x, axis):
    leaves = jax.tree.leaves(x)
    sequence = sorted(range(len(leaves)), key=lambda k: -leaves[k].size)
    width = (1, *leaves[sequence[0]].shape)[-1]
    lines = [
        jnp.pad(leaves[k].reshape(-1), (0, -leaves[k].size % width)).reshape(-1, width)
        for k in sequence
    ]
    both, at, found = (lax.all_gather(jnp.concatenate(lines), axis), 0, {})
    for k, line in zip(sequence, lines):
        slab = both[:, at : at + len(line)].reshape(len(both), -1)
        found[k] = slab[:, : leaves[k].size].reshape(-1, *leaves[k].shape)
        at += len(line)
    numbers = iter(range(len(leaves)))
    return jax.tree.map(lambda _: found[next(numbers)], x)


def entering(x, axes, combine, identity):
    before = start = neutral_like(x, identity)
    running = x
    for axis in reversed(axes):
        count, position = (lax.axis_size(axis), lax.axis_index(axis))
        pieces = gathered_once(
            jax.tree.map(
                lambda part, kind: part.astype(kind),
                running,
                (jnp.bfloat16, jnp.bfloat16, jnp.bfloat16, jnp.bfloat16),
            ),
            axis,
        )
        inside, running = (start, start)
        for k in range(count):
            passed = k < position
            running = combine(
                running, jax.tree.map(lambda part, own: part[k].astype(own.dtype), pieces, x)
            )
            inside = jax.tree.map(lambda new, old: jnp.where(passed, new, old), running, inside)
        before = combine(inside, before)
    return before


def shifted(x, axis, by):
    count = lax.axis_size(axis)
    pairs = [(i, i + by) for i in range(count) if 0 <= i + by < count]
    return lax.ppermute(x, axis, pairs)


def side_by_side(arrays, axis, dim, along):
    both = jnp.concatenate(arrays, axis=along)
    result, at, finished = (lax.all_gather(both, axis, axis=dim, tiled=True), 0, [])
    for a in arrays:
        finished.append(lax.slice_in_dim(result, at, at + a.shape[along], axis=along))
        at += a.shape[along]
    return tuple(finished)


def laid_out(tiles, dim):
    shape = list(tiles.shape[1:])
    shape[dim] *= tiles.shape[0]
    return jnp.moveaxis(tiles, 0, dim).reshape(shape)


def all_blocks(x, axes, sequence):
    tiles = x
    for k in sequence:
        tiles = lax.all_gather(tiles, axes[k])
    done = sequence[::-1]
    back = [done.index(k) for k in range(len(axes))]
    tiles = tiles.transpose(*back, *range(len(axes), tiles.ndim))
    return tiles.reshape(-1, *x.shape)


def gather_axes(x, axes, sequence, dim):
    return laid_out(all_blocks(x, axes, sequence), dim)


def gate_log_values(input_gate_logits, forget_gate_logits, forget_decay_offset):
    input_log_value = 15.0 * jnp.tanh(input_gate_logits / 15.0)
    forget_log_sigmoid = (
        jax.nn.log_sigmoid(15.0 * jnp.tanh(forget_gate_logits / 15.0)) + forget_decay_offset
    )
    return (input_log_value, forget_log_sigmoid)


def combine_states(earlier, later):
    total_one, memory_one, normer_one, running_one = earlier
    total_two, memory_two, normer_two, running_two = later
    joined = jnp.maximum(total_two + running_one, running_two)
    weight_one = jnp.exp(total_two + running_one - joined)
    weight_two = jnp.exp(running_two - joined)
    memory = weight_one[:, None, None] * memory_one + weight_two[:, None, None] * memory_two
    normer = weight_one[:, None] * normer_one + weight_two[:, None] * normer_two
    return (total_one + total_two, memory, normer, joined)


def local_step(state_carry, inputs):
    memory, normer, running = state_carry
    query_block, key_block, value_block, input_block, forget_block = inputs
    length = query_block.shape[0]
    highest = lax.Precision.DEFAULT
    query_scale = query_block.shape[2] ** (-0.5)
    causal = jnp.tril(jnp.ones((length, length), dtype=bool))[:, :, None]
    cumulative = jnp.cumsum(forget_block, axis=0)
    logits = cumulative[:, None, :] - cumulative[None, :, :] + input_block[None, :, :]
    logits = jnp.where(causal, logits, -jnp.inf)
    carried = cumulative + running[None, :]
    stable = jnp.maximum(carried, jnp.max(logits, axis=1))
    carry_weight = jnp.exp(carried - stable)
    raw = (
        jnp.einsum("thd,shd->tsh", query_block, key_block, preferred_element_type=jnp.float32)
        * query_scale
    )
    scores = raw * jnp.exp(logits - stable[:, None, :])
    scaled_query = query_block.astype(jnp.float32) * query_scale
    numerator = carry_weight[:, :, None] * jnp.einsum(
        "hvd,thd->thv", memory, scaled_query, precision=highest
    )
    numerator = numerator + jnp.einsum(
        "tsh,shv->thv", scores.astype(jnp.bfloat16), value_block, preferred_element_type=jnp.float32
    )
    denominator = carry_weight * jnp.einsum(
        "hd,thd->th", normer, scaled_query, precision=highest
    ) + jnp.sum(scores, axis=1)
    last_sum = cumulative[-1]
    weights_log = last_sum[None, :] - cumulative + input_block
    new_running = jnp.maximum(last_sum + running, jnp.max(weights_log, axis=0))
    decay_factor = jnp.exp(last_sum + running - new_running)
    weighted = (
        key_block.astype(jnp.float32) * jnp.exp(weights_log - new_running[None, :])[:, :, None]
    )
    memory = decay_factor[:, None, None] * memory + jnp.einsum(
        "shv,shd->hvd",
        value_block,
        weighted.astype(jnp.bfloat16),
        preferred_element_type=jnp.float32,
    )
    normer = decay_factor[:, None] * normer + jnp.sum(weighted, axis=0)
    return ((memory, normer, new_running), (numerator, denominator, stable))


def local(
    residual_entry_input,
    query_matrix_rows,
    key_matrix_rows,
    value_matrix_rows,
    output_gate_logits,
    input_gate_logits,
    forget_gate_logits,
    forget_decay_offset,
    head_norm_gain,
    cell_output_weight,
    feedforward_norm_gain,
    gate_up_weight,
    value_up_weight,
    gate_filter_taps,
    value_filter_taps,
    down_projection_weight,
):
    highest = lax.Precision.DEFAULT
    token_count = query_matrix_rows.shape[0]
    head_count = input_gate_logits.shape[1]
    key_width = query_matrix_rows.shape[1] // head_count
    value_width = value_matrix_rows.shape[1] // head_count
    query_scale = key_width ** (-0.5)
    queries_low = query_matrix_rows.reshape(token_count, head_count, key_width)
    keys_low = key_matrix_rows.reshape(token_count, head_count, key_width)
    values_low = value_matrix_rows.reshape(token_count, head_count, value_width)
    input_log_value, forget_log_sigmoid = gate_log_values(
        input_gate_logits, forget_gate_logits, forget_decay_offset
    )
    cumulative = jnp.cumsum(forget_log_sigmoid, axis=0)
    total_log = cumulative[-1]
    block_count = token_count // BLOCK

    def blocks(tensor):
        return tensor.reshape((block_count, BLOCK) + tensor.shape[1:])

    initial = (
        jnp.zeros((head_count, value_width, key_width), jnp.float32),
        jnp.zeros((head_count, key_width), jnp.float32),
        jnp.full((head_count,), neg_large, jnp.float32),
    )
    end_state, (numerator, denominator, stable) = lax.scan(
        local_step,
        initial,
        (
            blocks(queries_low),
            blocks(keys_low),
            blocks(values_low),
            blocks(input_log_value),
            blocks(forget_log_sigmoid),
        ),
    )
    end_memory, end_normer, end_running = end_state
    identity = (
        jnp.zeros((head_count,), jnp.float32),
        jnp.zeros((head_count, value_width, key_width), jnp.float32),
        jnp.zeros((head_count, key_width), jnp.float32),
        jnp.full((head_count,), neg_large, jnp.float32),
    )
    prefix = entering(
        (total_log, end_memory, end_normer, end_running), SP, combine_states, identity
    )
    numerator = numerator.reshape(token_count, head_count, value_width)
    denominator = denominator.reshape(token_count, head_count)
    stable = stable.reshape(token_count, head_count)
    _, prior_memory, prior_normer, prior_running = prefix
    scaled_query = queries_low.astype(jnp.float32) * query_scale
    prior_log = cumulative + prior_running[None, :]
    top_log = jnp.maximum(stable, prior_log)
    local_weight = jnp.exp(stable - top_log)
    prior_weight = jnp.exp(prior_log - top_log)
    numerator = local_weight[:, :, None] * numerator + prior_weight[:, :, None] * jnp.einsum(
        "hvd,thd->thv", prior_memory, scaled_query, precision=highest
    )
    denominator = local_weight * denominator + prior_weight * jnp.einsum(
        "hd,thd->th", prior_normer, scaled_query, precision=highest
    )
    memory_out = numerator / jnp.maximum(jnp.abs(denominator), jnp.exp(-top_log))[:, :, None]
    normed = (
        memory_out
        * lax.rsqrt(jnp.mean(memory_out * memory_out, axis=-1, keepdims=True) + eps)
        * head_norm_gain[None, :, :]
    )
    gated_rows = (
        normed.reshape(token_count, head_count * value_width)
        * jax.nn.sigmoid(output_gate_logits.astype(jnp.float32))
    ).astype(jnp.bfloat16)
    whole_out = lax.all_gather(cell_output_weight, "tp", axis=0, tiled=True)
    own_rows = lax.all_to_all(gated_rows, "tp", split_axis=0, concat_axis=1, tiled=True)
    mixed_rows = jnp.dot(own_rows, whole_out, preferred_element_type=jnp.float32)
    stream_wide = residual_entry_input.astype(jnp.float32) + mixed_rows
    stream = stream_wide.astype(jnp.bfloat16)
    stream_wide = lax.optimization_barrier(stream).astype(jnp.float32)
    normed_rows = (
        stream_wide
        * lax.rsqrt(jnp.mean(stream_wide * stream_wide, axis=-1, keepdims=True) + eps)
        * feedforward_norm_gain[None, :]
    ).astype(jnp.bfloat16)
    group_rows = lax.all_gather(normed_rows, "tp", axis=0, tiled=True)
    earlier_rows = shifted(group_rows[-2:], SP, 1)
    window = jnp.concatenate([earlier_rows, group_rows], axis=0)
    pieces = side_by_side((gate_up_weight, value_up_weight), SP, 0, 1)
    up_gate = jnp.dot(window, pieces[0], preferred_element_type=jnp.float32)
    up_value = jnp.dot(window, pieces[1], preferred_element_type=jnp.float32)
    conv_g = (
        gate_filter_taps[0][None, :] * up_gate[:-2]
        + gate_filter_taps[1][None, :] * up_gate[1:-1]
        + gate_filter_taps[2][None, :] * up_gate[2:]
    )
    conv_v = (
        value_filter_taps[0][None, :] * up_value[:-2]
        + value_filter_taps[1][None, :] * up_value[1:-1]
        + value_filter_taps[2][None, :] * up_value[2:]
    )
    hidden = (jax.nn.silu(conv_g) * conv_v).astype(jnp.bfloat16)
    whole_down = gather_axes(down_projection_weight, (("sp_0", "sp_1"), "sp_2"), (0, 1), 1)
    ffn_rows = lax.psum_scatter(
        jnp.dot(hidden, whole_down, preferred_element_type=jnp.float32).astype(jnp.bfloat16),
        "tp",
        scatter_dimension=0,
        tiled=True,
    ).astype(jnp.float32)
    return (stream_wide + ffn_rows).astype(jnp.bfloat16)


def solution(mesh):
    split = Mesh(mesh.devices.reshape(4, 4, 2, mesh.shape["tp"]), ("sp_0", "sp_1", "sp_2", "tp"))
    placed = (
        P(SP_TP, None),
        P(SP, "tp"),
        P(SP, "tp"),
        P(SP, "tp"),
        P(SP, "tp"),
        P(SP, "tp"),
        P(SP, "tp"),
        P(SP, "tp"),
        P("tp", None),
        P("tp", None),
        P(),
        P(SP, "tp"),
        P(SP, "tp"),
        P(None, "tp"),
        P(None, "tp"),
        P("tp", SP),
    )
    return jax.shard_map(
        local, mesh=split, in_specs=placed, out_specs=P(SP_TP, None), check_vma=False
    )
```

profile of v0, /device:TPU:1, one launch (start us, length us, event | category | flops | bytes accessed | tf_op | source)
XLA Modules:
  0.0 419.1 jit_solution(10256180526580571442)
XLA Ops:
  6.5 0.7 all-gather.14.cloned.1.call-update
  7.3 0.7 all-gather.20.cloned.1.call-update
  8.1 0.7 fusion.147
  9.1 1.3 reshape.1706
  10.7 0.9 reshape.1707
  11.7 2.0 reshape.1708
  13.6 102.5 %while.21 = (s32[]{:T(128)}, f32[2,256,128]{2,1,0:T(8,128)S(1)}, f32[2,128]{1,0:T(2,128)S(1)}, f32[2]{0:T(128)S(1)}, f32[8,128,2,256]{1,0,3,2:T(8,128)}, /*index...) while((s32[]{:T(128)}, f32[2,256,128]{2,1,0:T(8,128)S(1)}, ...), condition=%wide.region_6.7_spmd.clone, body=%wide.region_0.6_spmd.clone.sunk | while | flops 59952648 | bytes 4685610 | solution.py:202
  14.4 1.0 constant_dynamic-slice_fusion.6
  17.8 8.3 %dynamic_update_slice.19 = f32[8,128,2,256]{1,0,3,2:T(8,128)} dynamic-update-slice(f32[8,128,2,256]{1,0,3,2:T(8,128)} %get-tuple-element.428, f32[1,128,2,256]{1,0,3,2:T(1,128)S(1)} %copy.336, s32[]{:T(128)} %get-tuple-element.424, s32[]{:T(128)} %constant.38.clone.1..sunk, s32[]{:T(128)} %constant.38.clone.1..sunk, s32[]{:T(128)} %constant.38.clone.1..sunk) | dynamic-update-slice | bytes 524292 | tf_op jit(solution)/shard_map/while/body/jit(dynamic_update_index_in_dim)/dynamic_update_slice | solution.py:202
  27.3 1.0 constant_dynamic-slice_fusion.6
  30.7 8.2 %dynamic_update_slice.19 = f32[8,128,2,256]{1,0,3,2:T(8,128)} dynamic-update-slice(f32[8,128,2,256]{1,0,3,2:T(8,128)} %get-tuple-element.428, f32[1,128,2,256]{1,0,3,2:T(1,128)S(1)} %copy.336, s32[]{:T(128)} %get-tuple-element.424, s32[]{:T(128)} %constant.38.clone.1..sunk, s32[]{:T(128)} %constant.38.clone.1..sunk, s32[]{:T(128)} %constant.38.clone.1..sunk) | dynamic-update-slice | bytes 524292 | tf_op jit(solution)/shard_map/while/body/jit(dynamic_update_index_in_dim)/dynamic_update_slice | solution.py:202
  40.1 1.0 constant_dynamic-slice_fusion.6
  43.5 8.2 %dynamic_update_slice.19 = f32[8,128,2,256]{1,0,3,2:T(8,128)} dynamic-update-slice(f32[8,128,2,256]{1,0,3,2:T(8,128)} %get-tuple-element.428, f32[1,128,2,256]{1,0,3,2:T(1,128)S(1)} %copy.336, s32[]{:T(128)} %get-tuple-element.424, s32[]{:T(128)} %constant.38.clone.1..sunk, s32[]{:T(128)} %constant.38.clone.1..sunk, s32[]{:T(128)} %constant.38.clone.1..sunk) | dynamic-update-slice | bytes 524292 | tf_op jit(solution)/shard_map/while/body/jit(dynamic_update_index_in_dim)/dynamic_update_slice | solution.py:202
  52.9 1.0 constant_dynamic-slice_fusion.6
  56.3 8.2 %dynamic_update_slice.19 = f32[8,128,2,256]{1,0,3,2:T(8,128)} dynamic-update-slice(f32[8,128,2,256]{1,0,3,2:T(8,128)} %get-tuple-element.428, f32[1,128,2,256]{1,0,3,2:T(1,128)S(1)} %copy.336, s32[]{:T(128)} %get-tuple-element.424, s32[]{:T(128)} %constant.38.clone.1..sunk, s32[]{:T(128)} %constant.38.clone.1..sunk, s32[]{:T(128)} %constant.38.clone.1..sunk) | dynamic-update-slice | bytes 524292 | tf_op jit(solution)/shard_map/while/body/jit(dynamic_update_index_in_dim)/dynamic_update_slice | solution.py:202
  65.7 1.0 constant_dynamic-slice_fusion.6
  69.1 8.2 %dynamic_update_slice.19 = f32[8,128,2,256]{1,0,3,2:T(8,128)} dynamic-update-slice(f32[8,128,2,256]{1,0,3,2:T(8,128)} %get-tuple-element.428, f32[1,128,2,256]{1,0,3,2:T(1,128)S(1)} %copy.336, s32[]{:T(128)} %get-tuple-element.424, s32[]{:T(128)} %constant.38.clone.1..sunk, s32[]{:T(128)} %constant.38.clone.1..sunk, s32[]{:T(128)} %constant.38.clone.1..sunk) | dynamic-update-slice | bytes 524292 | tf_op jit(solution)/shard_map/while/body/jit(dynamic_update_index_in_dim)/dynamic_update_slice | solution.py:202
  78.5 1.0 constant_dynamic-slice_fusion.6
  81.9 8.2 %dynamic_update_slice.19 = f32[8,128,2,256]{1,0,3,2:T(8,128)} dynamic-update-slice(f32[8,128,2,256]{1,0,3,2:T(8,128)} %get-tuple-element.428, f32[1,128,2,256]{1,0,3,2:T(1,128)S(1)} %copy.336, s32[]{:T(128)} %get-tuple-element.424, s32[]{:T(128)} %constant.38.clone.1..sunk, s32[]{:T(128)} %constant.38.clone.1..sunk, s32[]{:T(128)} %constant.38.clone.1..sunk) | dynamic-update-slice | bytes 524292 | tf_op jit(solution)/shard_map/while/body/jit(dynamic_update_index_in_dim)/dynamic_update_slice | solution.py:202
  91.3 1.0 constant_dynamic-slice_fusion.6
  94.7 8.2 %dynamic_update_slice.19 = f32[8,128,2,256]{1,0,3,2:T(8,128)} dynamic-update-slice(f32[8,128,2,256]{1,0,3,2:T(8,128)} %get-tuple-element.428, f32[1,128,2,256]{1,0,3,2:T(1,128)S(1)} %copy.336, s32[]{:T(128)} %get-tuple-element.424, s32[]{:T(128)} %constant.38.clone.1..sunk, s32[]{:T(128)} %constant.38.clone.1..sunk, s32[]{:T(128)} %constant.38.clone.1..sunk) | dynamic-update-slice | bytes 524292 | tf_op jit(solution)/shard_map/while/body/jit(dynamic_update_index_in_dim)/dynamic_update_slice | solution.py:202
  104.1 1.0 constant_dynamic-slice_fusion.6
  107.5 8.2 %dynamic_update_slice.19 = f32[8,128,2,256]{1,0,3,2:T(8,128)} dynamic-update-slice(f32[8,128,2,256]{1,0,3,2:T(8,128)} %get-tuple-element.428, f32[1,128,2,256]{1,0,3,2:T(1,128)S(1)} %copy.336, s32[]{:T(128)} %get-tuple-element.424, s32[]{:T(128)} %constant.38.clone.1..sunk, s32[]{:T(128)} %constant.38.clone.1..sunk, s32[]{:T(128)} %constant.38.clone.1..sunk) | dynamic-update-slice | bytes 524292 | tf_op jit(solution)/shard_map/while/body/jit(dynamic_update_index_in_dim)/dynamic_update_slice | solution.py:202
  117.4 3.0 all-gather.5
  122.3 13.0 %all-gather.6 = bf16[4,516,128]{2,1,0:T(8,128)(2,1)S(1)} all-gather(bf16[1,516,128]{2,1,0:T(8,128)(2,1)S(1)} %maximum_bitcast_fusion.1), channel_id=3, replica_groups=mesh['sp_0'=4,'sp_1'=4,'sp_2'=2,'tp'=4] {'sp_1'}, dimensions={0}, use_global_device_ids=true | all-gather | bytes 660480 | tf_op jit(solution)/shard_map/all_gather | solution.py:28
  136.8 14.1 %all-gather.7 = bf16[4,516,128]{2,1,0:T(8,128)(2,1)S(1)} all-gather(bf16[1,516,128]{2,1,0:T(8,128)(2,1)S(1)} %maximum_bitcast_fusion.2), channel_id=4, replica_groups=mesh['sp_0'=4,'sp_1'=4,'sp_2'=2,'tp'=4] {'sp_0'}, dimensions={0}, use_global_device_ids=true | all-gather | bytes 660480 | tf_op jit(solution)/shard_map/all_gather | solution.py:28
  151.4 1.7 reshape.1638
  153.1 0.8 fusion.167
  154.1 1.3 fusion.47
  155.7 1.3 multiply_reduce_fusion
  157.2 1.9 copy.197
  159.2 2.5 multiply_convert_fusion
  161.7 14.4 %all_to_all.19 = bf16[4,256,512]{2,1,0:T(8,128)(2,1)S(1)} all-to-all(bf16[4,256,512]{2,1,0:T(8,128)(2,1)S(1)} %bitcast.610), channel_id=1, replica_groups=mesh['sp_0'=4,'sp_1'=4,'sp_2'=2,'tp'=4] {'tp'}, dimensions={0} | all-to-all | bytes 2097152 | tf_op jit(solution)/shard_map/all_to_all | solution.py:249
  176.6 5.7 %fusion.40 = bf16[256,2048]{1,0:T(8,128)(2,1)S(1)} fusion(bf16[256,2048]{0,1:T(8,128)(2,1)S(1)} %bitcast.606, bf16[2048,2048]{1,0:T(8,128)(2,1)} %all-gather.14.cloned.1.call-done, bf16[256,2048]{1,0:T(8,128)(2,1)S(1)} %copy-done), kind=kOutput, calls=%fused_computation.77 | convolution fusion | flops 2149056512 | bytes 11534336 | tf_op jit(solution)/shard_map/dot_general | solution.py:250
  182.7 1.3 fusion.43
  184.1 3.8 copy.246
  188.0 0.8 pad_maximum_fusion.3
  188.9 45.1 %all-gather.16.cloned.1.call-done = bf16[1024,2048]{1,0:T(8,128)(2,1)} async-done(((bf16[256,2048]{1,0:T(8,128)(2,1)}), bf16[1024,2048]{1,0:T(8,128)(2,1)}) %all-gather.16.cloned.1.call-update) | async-done | bytes 4194320 | tf_op jit(solution)/shard_map/all_gather | solution.py:259
  234.0 0.8 slice.352
  234.8 4.0 collective-permute-start
  238.9 16.3 %all-gather.22.cloned.1.call-done = bf16[32,1408,64]{1,0,2:T(8,128)(2,1)} async-done(((bf16[16,1408,64]{1,0,2:T(8,128)(2,1)}), bf16[32,1408,64]{1,0,2:T(8,128)(2,1)}) %all-gather.22.cloned.1.call-update) | async-done | bytes 5767184 | tf_op jit(solution)/shard_map/all_gather | solution.py:85
  255.2 7.0 %copy.200 = bf16[16,2,1408,64]{2,3,1,0:T(8,128)(2,1)} copy(bf16[16,2,1408,64]{2,0,1,3:T(8,128)(2,1)} %bitcast.607) | data formatting | bytes 11534336 | tf_op jit(solution)/shard_map/transpose | solution.py:88
  262.2 56.7 %all-gather.18.cloned.1.call-done = bf16[2048,2816]{1,0:T(8,128)(2,1)} async-done(((bf16[64,2816]{1,0:T(8,128)(2,1)}), bf16[2048,2816]{1,0:T(8,128)(2,1)}) %all-gather.18.cloned.1.call-update) | async-done | bytes 11534352 | tf_op jit(solution)/shard_map/all_gather | solution.py:69
  318.9 11.9 %fusion.37 = f32[1026,1408]{1,0:T(8,128)} fusion(bf16[2048,2816]{1,0:T(8,128)(2,1)} %all-gather.18.cloned.1.call-done, bf16[1024,2048]{1,0:T(8,128)(2,1)} %all-gather.16.cloned.1.call-done, bf16[2,2048]{1,0:T(2,128)(2,1)S(1)} %collective-permute-done), kind=kOutput, calls=%fused_computation.69 | convolution fusion | flops 5925519360 | bytes 15748096 | tf_op jit(solution)/shard_map/dot_general | solution.py:263
  330.9 8.7 %fusion.33 = f32[1026,1408]{1,0:T(8,128)} fusion(bf16[2048,2816]{1,0:T(8,128)(2,1)S(1)} %copy-done.13, bf16[1024,2048]{1,0:T(8,128)(2,1)S(1)} %copy-done.12, bf16[2,2048]{1,0:T(2,128)(2,1)S(1)} %collective-permute-done), kind=kOutput, calls=%fused_computation.62 | convolution fusion | flops 5925519360 | bytes 15748096 | tf_op jit(solution)/shard_map/dot_general | solution.py:264
  339.5 24.1 %convolution_convert_fusion = bf16[1024,2048]{1,0:T(8,128)(2,1)} fusion(bf16[1408,2048]{0,1:T(8,128)(2,1)} %bitcast.608, f32[1026,1408]{1,0:T(8,128)} %fusion.33, f32[1026,1408]{1,0:T(8,128)} %fusion.37, f32[1408]{0:T(1024)S(1)} %get-tuple-element.181, f32[1408]{0:T(1024)S(1)} %get-tuple-element.182, f32[1408]{0:T(1024)S(1)} %get-tuple-element.180, ...), kind=kOutput, calls=%fused_computation.72 | convolution fusion | flops 5930745856 | bytes 44598272 | tf_op jit(solution)/shard_map/dot_general | solution.py:278
  363.7 46.0 %reduce-scatter.2.cloned.1.call-done = bf16[256,2048]{1,0:T(8,128)(2,1)} async-done(((bf16[1024,2048]{1,0:T(8,128)(2,1)}), bf16[256,2048]{1,0:T(8,128)(2,1)}) %reduce-scatter.2.cloned.1.call-update) | async-done | bytes 1048592 | tf_op jit(solution)/shard_map/reduce_scatter | solution.py:277
  409.7 2.6 fusion.44
  (341 shorter events, 35.1 us)
Async XLA Ops:
  6.5 3.9 copy-start.10
  6.5 4.2 copy-start.1
  6.5 170.0 %all-gather.14.cloned.1.call-start = ((), (), s32[]{:S(2)}) async-start(), calls=%async_computation.2 | async-start | bytes 10485760 | tf_op jit(solution)/shard_map/all_gather | solution.py:248
  7.3 176.8 %all-gather.20.cloned.1.call-start = ((), (), s32[]{:S(2)}) async-start(), calls=%async_computation.6 | async-start | bytes 3063808 | tf_op jit(solution)/shard_map/all_gather | solution.py:85
  8.0 226.0 %all-gather.16.cloned.1.call-start = ((), (), s32[]{:S(2)}) async-start(), calls=%async_computation.3 | async-start | bytes 5242880 | tf_op jit(solution)/shard_map/all_gather | solution.py:259
  116.1 34.9 %copy-start.4 = (f32[8,128,2]{2,1,0:T(8,128)S(1)}, f32[8,128,2]{2,1,0:T(8,128)}, u32[]{:S(2)}) copy-start(f32[8,128,2]{2,1,0:T(8,128)} %get-tuple-element.72) | copy-start | bytes 24580
  116.1 35.1 %copy-start.3 = (f32[8,128,2]{2,1,0:T(8,128)S(1)}, f32[8,128,2]{2,1,0:T(8,128)}, u32[]{:S(2)}) copy-start(f32[8,128,2]{2,1,0:T(8,128)} %get-tuple-element.77) | copy-start | bytes 24580
  153.1 2.6 copy-start.2
  155.7 1.3 copy-start.11
  159.2 17.4 %copy-start = (bf16[256,2048]{1,0:T(8,128)(2,1)S(1)}, bf16[256,2048]{1,0:T(8,128)(2,1)}, u32[]{:S(2)}) copy-start(bf16[256,2048]{1,0:T(8,128)(2,1)} %param.18) | copy-start | bytes 3145732
  176.6 6.0 %copy-start.9 = (f32[2048]{0:T(1024)S(1)}, f32[2048]{0:T(1024)}, u32[]{:S(2)}) copy-start(f32[2048]{0:T(1024)} %param.28) | copy-start | bytes 24580
  184.0 71.2 %all-gather.22.cloned.1.call-start = ((), (), s32[]{:S(2)}) async-start(), calls=%async_computation.7 | async-start | bytes 8650752 | tf_op jit(solution)/shard_map/all_gather | solution.py:85
  184.0 4.0 copy-start.5
  184.0 4.0 copy-start.6
  184.1 54.8 %copy-start.7 = (f32[3,1408]{1,0:T(4,128)S(1)}, f32[3,1408]{1,0:T(4,128)}, u32[]{:S(2)}) copy-start(f32[3,1408]{1,0:T(4,128)} %param.32) | copy-start | bytes 50692
  184.1 54.8 %copy-start.8 = (f32[3,1408]{1,0:T(4,128)S(1)}, f32[3,1408]{1,0:T(4,128)}, u32[]{:S(2)}) copy-start(f32[3,1408]{1,0:T(4,128)} %param.31) | copy-start | bytes 50692
  187.9 131.0 %all-gather.18.cloned.1.call-start = ((), (), s32[]{:S(2)}) async-start(), calls=%async_computation.4 | async-start | bytes 11894784 | tf_op jit(solution)/shard_map/all_gather | solution.py:69
  188.8 220.8 %reduce-scatter.2.cloned.1.call-start = ((), (), s32[]{:S(2)}) async-start(), calls=%async_computation.5 | async-start | bytes 5242880 | tf_op jit(solution)/shard_map/reduce_scatter | solution.py:277
  234.8 27.4 %collective-permute-start = (bf16[2,2048]{1,0:T(2,128)(2,1)S(1)}, bf16[2,2048]{1,0:T(2,128)(2,1)S(1)}, u32[]{:S(2)}, u32[]{:S(2)}) collective-permute-start(bf16[2,2048]{1,0:T(2,128)(2,1)S(1)} %slice.352), channel_id=1, source_target_pairs={{0,4},{4,8},{8,12},{12,16},{16,20},{20,24},{24,28},{28,32},{32,36}... | collective-permute-start | bytes 24584 | tf_op jit(solution)/shard_map/ppermute | solution.py:64
  318.9 11.9 %copy-start.12 = (bf16[1024,2048]{1,0:T(8,128)(2,1)S(1)}, bf16[1024,2048]{1,0:T(8,128)(2,1)}, u32[]{:S(2)}) copy-start(bf16[1024,2048]{1,0:T(8,128)(2,1)} %all-gather.16.cloned.1.call-done) | copy-start | bytes 12582916
  318.9 11.9 %copy-start.13 = (bf16[2048,2816]{1,0:T(8,128)(2,1)S(1)}, bf16[2048,2816]{1,0:T(8,128)(2,1)}, u32[]{:S(2)}) copy-start(bf16[2048,2816]{1,0:T(8,128)(2,1)} %all-gather.18.cloned.1.call-done) | copy-start | bytes 34603012
Sparse Core Ops, SparseCore 0:
  9.0 86.0 all-gather.13
  97.3 51.0 all-gather.19
  184.1 49.8 all-gather.15
  235.5 19.6 all-gather.21
  257.3 61.5 all-gather.17
  363.8 45.7 reduce-scatter.1
where the time goes:
time: 421 us; the launch traced here: 419 us
  waiting for transfers between devices  166 us (39%)
  local copies, waits for them, and re-layouts  105 us (25%)
  matrix products  62 us (15%)
  blocking collectives  44.6 us (11%)
  other arithmetic  23.2 us (6%)
  between operations  14.1 us (3%)
  starting transfers between devices  4.22 us (1%)
    dynamic_update_slice x16, local copies, waits for them, and re-layouts, local(): lax.scan(local_step, initial, (blocks(queries_low), blocks(keys_low), blo...  66.9 us
    all_gather x1, waiting for transfers between devices, side_by_side(): lax.all_gather(both, axis, axis=dim, tiled=True)  56.7 us
    reduce_scatter x1, waiting for transfers between devices, local(): lax.psum_scatter(jnp.dot(hidden, whole_down, preferred_element_type=jnp.f...  46 us
    all_gather x1, waiting for transfers between devices, local(): group_rows = lax.all_gather(normed_rows, 'tp', axis=0, tiled=True)  45.1 us
    all_gather x3, blocking collectives, gathered_once(): both, at, found = (lax.all_gather(jnp.concatenate(lines), axis), 0, {})  30.2 us
    dot_general x1, matrix products, local(): jnp.dot(hidden, whole_down, preferred_element_type=jnp.float32)  24.1 us
    all_gather x2, waiting for transfers between devices, all_blocks(): tiles = lax.all_gather(tiles, axes[k])  16.3 us
    all_to_all x1, blocking collectives, local(): lax.all_to_all(gated_rows, 'tp', split_axis=0, concat_axis=1, tiled=True)  14.4 us
  transfers between devices with their start and end apart: 7, of which 4 were waited for; matrix products, arithmetic and copies ran while one was open for 34% of the time, Pallas kernels for 0%

commit v1 on v0

--- a/solution.py
+++ b/solution.py
@@ -9,6 +9,16 @@
 SP_TP = ("sp_0", "sp_1", "sp_2", "tp")
 eps = 1e-06
 neg_large = -1e30
+
+
+def pass_along(x, axis, dim):
+    size = lax.axis_size(axis)
+    current, blocks = (x, [x])
+    for _ in range(size - 1):
+        current = lax.ppermute(current, axis, [(i, (i + 1) % size) for i in range(size)])
+        blocks.insert(0, current)
+    line = jnp.concatenate(blocks, axis=dim)
+    return jnp.roll(line, (lax.axis_index(axis) + 1) * x.shape[dim], axis=dim)
 
 
 def neutral_like(x, identity):
@@ -256,7 +266,7 @@
         * lax.rsqrt(jnp.mean(stream_wide * stream_wide, axis=-1, keepdims=True) + eps)
         * feedforward_norm_gain[None, :]
     ).astype(jnp.bfloat16)
-    group_rows = lax.all_gather(normed_rows, "tp", axis=0, tiled=True)
+    group_rows = pass_along(normed_rows, "tp", 0)
     earlier_rows = shifted(group_rows[-2:], SP, 1)
     window = jnp.concatenate([earlier_rows, group_rows], axis=0)
     pieces = side_by_side((gate_up_weight, value_up_weight), SP, 0, 1)

time: 421 us -> 419 us (level)
  waiting for transfers between devices: 166 us -> 151 us
  starting transfers between devices: 4.22 us -> 13.5 us
  local copies, waits for them, and re-layouts: 105 us -> 112 us
  blocking collectives: 44.6 us -> 40 us
    all_gather x1, waiting for transfers between devices: 56.7 us -> 0.01 us  [side_by_side(): lax.all_gather(both, axis, axis=dim, tiled=True)]
    ppermute x0 -> x3, waiting for transfers between devices: none -> 54.1 us  [pass_along(): lax.ppermute(current, axis, [(i, (i + 1) % size) for i in range(size)])]
    all_gather x1 -> x0, waiting for transfers between devices: 45.1 us -> none  [local(): group_rows = lax.all_gather(normed_rows, 'tp', axis=0, tiled=True)]
    all_gather x2, waiting for transfers between devices: 16.3 us -> 51.1 us  [all_blocks(): tiles = lax.all_gather(tiles, axes[k])]
    ppermute x1, starting transfers between devices: 4.02 us -> 12.7 us  [shifted(): return lax.ppermute(x, axis, pairs)]
    all_gather x3, blocking collectives: 30.2 us -> 25.8 us  [gathered_once(): both, at, found = (lax.all_gather(jnp.concatenate(lines), axis), 0, {})]
  transfers between devices with their start and end apart: 7 -> 9, of which waited for: 4 -> 5; matrix products, arithmetic and copies ran while one was open for 34% -> 36% of each run, Pallas kernels for 0% -> 0%
where the time goes in v1:
time: 419 us; the launch traced here: 417 us
  waiting for transfers between devices  151 us (36%)
  local copies, waits for them, and re-layouts  112 us (27%)
  matrix products  63.1 us (15%)
  blocking collectives  40 us (10%)
  other arithmetic  22 us (5%)
  between operations  13.7 us (3%)
  starting transfers between devices  13.5 us (3%)
    dynamic_update_slice x16, local copies, waits for them, and re-layouts, local(): lax.scan(local_step, initial, (blocks(queries_low), blocks(keys_low), blo...  66.7 us
    ppermute x3, waiting for transfers between devices, pass_along(): lax.ppermute(current, axis, [(i, (i + 1) % size) for i in range(size)])  54.1 us
    all_gather x2, waiting for transfers between devices, all_blocks(): tiles = lax.all_gather(tiles, axes[k])  51.1 us
    reduce_scatter x1, waiting for transfers between devices, local(): lax.psum_scatter(jnp.dot(hidden, whole_down, preferred_element_type=jnp.f...  44.7 us
    all_gather x3, blocking collectives, gathered_once(): both, at, found = (lax.all_gather(jnp.concatenate(lines), axis), 0, {})  25.8 us
    dot_general x1, matrix products, local(): jnp.dot(hidden, whole_down, preferred_element_type=jnp.float32)  24.2 us
    all_to_all x1, blocking collectives, local(): lax.all_to_all(gated_rows, 'tp', split_axis=0, concat_axis=1, tiled=True)  14.2 us
    ppermute x1, starting transfers between devices, shifted(): return lax.ppermute(x, axis, pairs)  12.7 us
  transfers between devices with their start and end apart: 9, of which 5 were waited for; matrix products, arithmetic and copies ran while one was open for 36% of the time, Pallas kernels for 0%

profile of v1, /device:TPU:1, one launch (start us, length us, event | category | flops | bytes accessed | tf_op | source)
XLA Modules:
  0.0 416.8 jit_solution(6871465984757861809)
XLA Ops:
  8.1 51.1 %all-gather.17.cloned.1.call-done = bf16[22528,64]{0,1:T(8,128)(2,1)} async-done(((bf16[1408,64]{0,1:T(8,128)(2,1)}), bf16[22528,64]{0,1:T(8,128)(2,1)}) %all-gather.17.cloned.1.call-update) | async-done | bytes 2883600 | tf_op jit(solution)/shard_map/all_gather | solution.py:95
  59.2 3.9 copy.246
  63.1 0.8 pad_maximum_fusion.3
  64.3 1.3 reshape.1706
  65.9 0.9 reshape.1707
  66.9 2.0 reshape.1708
  68.8 102.3 %while.21 = (s32[]{:T(128)}, f32[2,256,128]{2,1,0:T(8,128)S(1)}, f32[2,128]{1,0:T(2,128)S(1)}, f32[2]{0:T(128)S(1)}, f32[8,128,2,256]{1,0,3,2:T(8,128)}, /*index...) while((s32[]{:T(128)}, f32[2,256,128]{2,1,0:T(8,128)S(1)}, ...), condition=%wide.region_6.7_spmd.clone, body=%wide.region_0.6_spmd.clone.sunk | while | flops 59952648 | bytes 4685610 | solution.py:212
  69.6 1.0 constant_dynamic-slice_fusion.8
  73.0 8.2 %dynamic_update_slice.19 = f32[8,128,2,256]{1,0,3,2:T(8,128)} dynamic-update-slice(f32[8,128,2,256]{1,0,3,2:T(8,128)} %get-tuple-element.428, f32[1,128,2,256]{1,0,3,2:T(1,128)S(1)} %copy.336, s32[]{:T(128)} %get-tuple-element.424, s32[]{:T(128)} %constant.93.clone.1..sunk, s32[]{:T(128)} %constant.93.clone.1..sunk, s32[]{:T(128)} %constant.93.clone.1..sunk) | dynamic-update-slice | bytes 524292 | tf_op jit(solution)/shard_map/while/body/jit(dynamic_update_index_in_dim)/dynamic_update_slice | solution.py:212
  82.4 1.0 constant_dynamic-slice_fusion.8
  85.8 8.2 %dynamic_update_slice.19 = f32[8,128,2,256]{1,0,3,2:T(8,128)} dynamic-update-slice(f32[8,128,2,256]{1,0,3,2:T(8,128)} %get-tuple-element.428, f32[1,128,2,256]{1,0,3,2:T(1,128)S(1)} %copy.336, s32[]{:T(128)} %get-tuple-element.424, s32[]{:T(128)} %constant.93.clone.1..sunk, s32[]{:T(128)} %constant.93.clone.1..sunk, s32[]{:T(128)} %constant.93.clone.1..sunk) | dynamic-update-slice | bytes 524292 | tf_op jit(solution)/shard_map/while/body/jit(dynamic_update_index_in_dim)/dynamic_update_slice | solution.py:212
  95.2 1.0 constant_dynamic-slice_fusion.8
  98.6 8.2 %dynamic_update_slice.19 = f32[8,128,2,256]{1,0,3,2:T(8,128)} dynamic-update-slice(f32[8,128,2,256]{1,0,3,2:T(8,128)} %get-tuple-element.428, f32[1,128,2,256]{1,0,3,2:T(1,128)S(1)} %copy.336, s32[]{:T(128)} %get-tuple-element.424, s32[]{:T(128)} %constant.93.clone.1..sunk, s32[]{:T(128)} %constant.93.clone.1..sunk, s32[]{:T(128)} %constant.93.clone.1..sunk) | dynamic-update-slice | bytes 524292 | tf_op jit(solution)/shard_map/while/body/jit(dynamic_update_index_in_dim)/dynamic_update_slice | solution.py:212
  108.0 1.0 constant_dynamic-slice_fusion.8
  111.4 8.2 %dynamic_update_slice.19 = f32[8,128,2,256]{1,0,3,2:T(8,128)} dynamic-update-slice(f32[8,128,2,256]{1,0,3,2:T(8,128)} %get-tuple-element.428, f32[1,128,2,256]{1,0,3,2:T(1,128)S(1)} %copy.336, s32[]{:T(128)} %get-tuple-element.424, s32[]{:T(128)} %constant.93.clone.1..sunk, s32[]{:T(128)} %constant.93.clone.1..sunk, s32[]{:T(128)} %constant.93.clone.1..sunk) | dynamic-update-slice | bytes 524292 | tf_op jit(solution)/shard_map/while/body/jit(dynamic_update_index_in_dim)/dynamic_update_slice | solution.py:212
  120.8 1.0 constant_dynamic-slice_fusion.8
  124.2 8.2 %dynamic_update_slice.19 = f32[8,128,2,256]{1,0,3,2:T(8,128)} dynamic-update-slice(f32[8,128,2,256]{1,0,3,2:T(8,128)} %get-tuple-element.428, f32[1,128,2,256]{1,0,3,2:T(1,128)S(1)} %copy.336, s32[]{:T(128)} %get-tuple-element.424, s32[]{:T(128)} %constant.93.clone.1..sunk, s32[]{:T(128)} %constant.93.clone.1..sunk, s32[]{:T(128)} %constant.93.clone.1..sunk) | dynamic-update-slice | bytes 524292 | tf_op jit(solution)/shard_map/while/body/jit(dynamic_update_index_in_dim)/dynamic_update_slice | solution.py:212
  133.6 1.0 constant_dynamic-slice_fusion.8
  137.0 8.2 %dynamic_update_slice.19 = f32[8,128,2,256]{1,0,3,2:T(8,128)} dynamic-update-slice(f32[8,128,2,256]{1,0,3,2:T(8,128)} %get-tuple-element.428, f32[1,128,2,256]{1,0,3,2:T(1,128)S(1)} %copy.336, s32[]{:T(128)} %get-tuple-element.424, s32[]{:T(128)} %constant.93.clone.1..sunk, s32[]{:T(128)} %constant.93.clone.1..sunk, s32[]{:T(128)} %constant.93.clone.1..sunk) | dynamic-update-slice | bytes 524292 | tf_op jit(solution)/shard_map/while/body/jit(dynamic_update_index_in_dim)/dynamic_update_slice | solution.py:212
  146.3 1.0 constant_dynamic-slice_fusion.8
  149.7 8.2 %dynamic_update_slice.19 = f32[8,128,2,256]{1,0,3,2:T(8,128)} dynamic-update-slice(f32[8,128,2,256]{1,0,3,2:T(8,128)} %get-tuple-element.428, f32[1,128,2,256]{1,0,3,2:T(1,128)S(1)} %copy.336, s32[]{:T(128)} %get-tuple-element.424, s32[]{:T(128)} %constant.93.clone.1..sunk, s32[]{:T(128)} %constant.93.clone.1..sunk, s32[]{:T(128)} %constant.93.clone.1..sunk) | dynamic-update-slice | bytes 524292 | tf_op jit(solution)/shard_map/while/body/jit(dynamic_update_index_in_dim)/dynamic_update_slice | solution.py:212
  159.1 1.0 constant_dynamic-slice_fusion.8
  162.6 8.2 %dynamic_update_slice.19 = f32[8,128,2,256]{1,0,3,2:T(8,128)} dynamic-update-slice(f32[8,128,2,256]{1,0,3,2:T(8,128)} %get-tuple-element.428, f32[1,128,2,256]{1,0,3,2:T(1,128)S(1)} %copy.336, s32[]{:T(128)} %get-tuple-element.424, s32[]{:T(128)} %constant.93.clone.1..sunk, s32[]{:T(128)} %constant.93.clone.1..sunk, s32[]{:T(128)} %constant.93.clone.1..sunk) | dynamic-update-slice | bytes 524292 | tf_op jit(solution)/shard_map/while/body/jit(dynamic_update_index_in_dim)/dynamic_update_slice | solution.py:212
  172.5 2.9 all-gather.5
  177.2 12.4 %all-gather.6 = bf16[4,516,128]{2,1,0:T(8,128)(2,1)S(1)} all-gather(bf16[1,516,128]{2,1,0:T(8,128)(2,1)S(1)} %maximum_bitcast_fusion.1), channel_id=3, replica_groups=mesh['sp_0'=4,'sp_1'=4,'sp_2'=2,'tp'=4] {'sp_1'}, dimensions={0}, use_global_device_ids=true | all-gather | bytes 660480 | tf_op jit(solution)/shard_map/all_gather | solution.py:38
  191.0 10.5 %all-gather.7 = bf16[4,516,128]{2,1,0:T(8,128)(2,1)S(1)} all-gather(bf16[1,516,128]{2,1,0:T(8,128)(2,1)S(1)} %maximum_bitcast_fusion.2), channel_id=4, replica_groups=mesh['sp_0'=4,'sp_1'=4,'sp_2'=2,'tp'=4] {'sp_0'}, dimensions={0}, use_global_device_ids=true | all-gather | bytes 660480 | tf_op jit(solution)/shard_map/all_gather | solution.py:38
  201.6 1.4 copy.213
  203.0 1.2 copy.214
  204.2 1.7 reshape.1638
  206.8 1.3 fusion.47
  208.4 2.3 multiply_reduce_fusion
  211.0 1.9 copy.197
  212.9 2.6 multiply_convert_fusion
  215.5 14.2 %all_to_all.19 = bf16[4,256,512]{2,1,0:T(8,128)(2,1)S(1)} all-to-all(bf16[4,256,512]{2,1,0:T(8,128)(2,1)S(1)} %bitcast.610), channel_id=1, replica_groups=mesh['sp_0'=4,'sp_1'=4,'sp_2'=2,'tp'=4] {'tp'}, dimensions={0} | all-to-all | bytes 2097152 | tf_op jit(solution)/shard_map/all_to_all | solution.py:259
  230.3 5.7 %fusion.40 = bf16[256,2048]{1,0:T(8,128)(2,1)S(1)} fusion(bf16[256,2048]{0,1:T(8,128)(2,1)S(1)} %bitcast.606, bf16[2048,2048]{1,0:T(8,128)(2,1)} %all-gather.13.cloned.1.call-done, bf16[256,2048]{1,0:T(8,128)(2,1)S(1)} %copy-done.1), kind=kOutput, calls=%fused_computation.77 | convolution fusion | flops 2149056512 | bytes 11534336 | tf_op jit(solution)/shard_map/dot_general | solution.py:260
  237.3 18.0 %collective-permute-done = bf16[256,2048]{1,0:T(8,128)(2,1)S(1)} collective-permute-done((bf16[256,2048]{1,0:T(8,128)(2,1)S(1)}, bf16[256,2048]{1,0:T(8,128)(2,1)S(1)}, u32[]{:S(2)}, u32[]{:S(2)}) %collective-permute-start) | collective-permute-done | bytes 1048608 | tf_op jit(solution)/shard_map/ppermute | solution.py:18
  255.3 21.6 %collective-permute-done.1 = bf16[256,2048]{1,0:T(8,128)(2,1)S(1)} collective-permute-done((bf16[256,2048]{1,0:T(8,128)(2,1)S(1)}, bf16[256,2048]{1,0:T(8,128)(2,1)S(1)}, u32[]{:S(2)}, u32[]{:S(2)}) %collective-permute-start.1) | collective-permute-done | bytes 1048608 | tf_op jit(solution)/shard_map/ppermute | solution.py:18
  277.0 7.1 %copy.200 = bf16[16,2,1408,64]{2,3,1,0:T(8,128)(2,1)} copy(bf16[16,2,1408,64]{2,0,1,3:T(8,128)(2,1)} %bitcast.607) | data formatting | bytes 11534336 | tf_op jit(solution)/shard_map/transpose | solution.py:98
  284.1 14.5 %collective-permute-done.2 = bf16[256,2048]{1,0:T(8,128)(2,1)} collective-permute-done((bf16[256,2048]{1,0:T(8,128)(2,1)S(1)}, bf16[256,2048]{1,0:T(8,128)(2,1)}, u32[]{:S(2)}, u32[]{:S(2)}) %collective-permute-start.2) | collective-permute-done | bytes 1048608 | tf_op jit(solution)/shard_map/ppermute | solution.py:18
  298.6 1.3 constant_dynamic-update-slice_fusion.7
  300.4 1.3 constant_dynamic-update-slice_fusion.3
  302.2 12.7 %collective-permute-start.3 = (bf16[2,2048]{1,0:T(2,128)(2,1)S(1)}, bf16[2,2048]{1,0:T(2,128)(2,1)S(1)}, u32[]{:S(2)}, u32[]{:S(2)}) collective-permute-start(bf16[2,2048]{1,0:T(2,128)(2,1)S(1)} %constant_dynamic-slice_fusion.3), channel_id=1, source_target_pairs={{0,4},{4,8},{8,12},{12,16},{16,20},{20,24},{24,28},{28,32},{32,36}... | collective-permute-start | bytes 24584 | tf_op jit(solution)/shard_map/ppermute | solution.py:74
  314.9 3.2 constant_dynamic-slice_fusion.4
  318.1 12.0 %fusion.37 = f32[1026,1408]{1,0:T(8,128)} fusion(bf16[2048,2816]{1,0:T(8,128)(2,1)} %all-gather.15.cloned.1.call-done, bf16[1024,2048]{1,0:T(8,128)(2,1)} %constant_dynamic-slice_fusion.4, bf16[2,2048]{1,0:T(2,128)(2,1)S(1)} %collective-permute-done.3), kind=kOutput, calls=%fused_computation.69 | convolution fusion | flops 5925519360 | bytes 15748096 | tf_op jit(solution)/shard_map/dot_general | solution.py:273
  330.1 8.7 %fusion.33 = f32[1026,1408]{1,0:T(8,128)} fusion(bf16[2048,2816]{1,0:T(8,128)(2,1)S(1)} %copy-done.12, bf16[1024,2048]{1,0:T(8,128)(2,1)S(1)} %copy-done, bf16[2,2048]{1,0:T(2,128)(2,1)S(1)} %collective-permute-done.3), kind=kOutput, calls=%fused_computation.62 | convolution fusion | flops 5925519360 | bytes 15748096 | tf_op jit(solution)/shard_map/dot_general | solution.py:274
  338.8 24.2 %convolution_convert_fusion = bf16[1024,2048]{1,0:T(8,128)(2,1)} fusion(bf16[1408,2048]{0,1:T(8,128)(2,1)} %bitcast.608, f32[1026,1408]{1,0:T(8,128)} %fusion.33, f32[1026,1408]{1,0:T(8,128)} %fusion.37, f32[1408]{0:T(1024)S(1)} %get-tuple-element.181, f32[1408]{0:T(1024)S(1)} %get-tuple-element.182, f32[1408]{0:T(1024)S(1)} %get-tuple-element.180, ...), kind=kOutput, calls=%fused_computation.72 | convolution fusion | flops 5930745856 | bytes 44598272 | tf_op jit(solution)/shard_map/dot_general | solution.py:288
  363.0 44.7 %reduce-scatter.2.cloned.1.call-done = bf16[256,2048]{1,0:T(8,128)(2,1)} async-done(((bf16[1024,2048]{1,0:T(8,128)(2,1)}), bf16[256,2048]{1,0:T(8,128)(2,1)}) %reduce-scatter.2.cloned.1.call-update) | async-done | bytes 1048592 | tf_op jit(solution)/shard_map/reduce_scatter | solution.py:287
  407.7 2.6 fusion.44
  (351 shorter events, 38.5 us)
Async XLA Ops:
  6.5 56.6 %copy-start.4 = (bf16[64,1408]{1,0:T(8,128)(2,1)S(1)}, bf16[64,1408]{1,0:T(8,128)(2,1)}, u32[]{:S(2)}) copy-start(bf16[64,1408]{1,0:T(8,128)(2,1)} %param.29) | copy-start | bytes 540676
  6.5 56.6 %copy-start.3 = (bf16[64,1408]{1,0:T(8,128)(2,1)S(1)}, bf16[64,1408]{1,0:T(8,128)(2,1)}, u32[]{:S(2)}) copy-start(bf16[64,1408]{1,0:T(8,128)(2,1)} %param.30) | copy-start | bytes 540676
  6.5 52.6 %all-gather.17.cloned.1.call-start = ((), (), s32[]{:S(2)}) async-start(), calls=%async_computation.5 | async-start | bytes 3063808 | tf_op jit(solution)/shard_map/all_gather | solution.py:95
  7.3 56.8 %copy-start.8 = (f32[1024,2]{0,1:T(2,128)S(1)}, f32[1024,2]{0,1:T(2,128)}, u32[]{:S(2)}) copy-start(f32[1024,2]{0,1:T(2,128)} %param.25) | copy-start | bytes 24580
  7.3 56.8 %copy-start.9 = (f32[1024,2]{0,1:T(2,128)S(1)}, f32[1024,2]{0,1:T(2,128)}, u32[]{:S(2)}) copy-start(f32[1024,2]{0,1:T(2,128)} %param.24) | copy-start | bytes 24580
  7.3 223.0 %all-gather.13.cloned.1.call-start = ((), (), s32[]{:S(2)}) async-start(), calls=%async_computation.2 | async-start | bytes 10485760 | tf_op jit(solution)/shard_map/all_gather | solution.py:258
  8.0 269.0 %all-gather.19.cloned.1.call-start = ((), (), s32[]{:S(2)}) async-start(), calls=%async_computation.6 | async-start | bytes 8650752 | tf_op jit(solution)/shard_map/all_gather | solution.py:95
  59.2 6.5 %copy-start.10 = (f32[1024,2]{0,1:T(2,128)S(1)}, f32[1024,2]{0,1:T(2,128)}, u32[]{:S(2)}) copy-start(f32[1024,2]{0,1:T(2,128)} %param.23) | copy-start | bytes 24580
  59.2 6.8 %copy-start.2 = (bf16[1024,256]{1,0:T(8,128)(2,1)S(1)}, bf16[1024,256]{1,0:T(8,128)(2,1)}, u32[]{:S(2)}) copy-start(bf16[1024,256]{1,0:T(8,128)(2,1)} %param.20) | copy-start | bytes 1572868
  63.0 255.1 %all-gather.15.cloned.1.call-start = ((), (), s32[]{:S(2)}) async-start(), calls=%async_computation.3 | async-start | bytes 11894784 | tf_op jit(solution)/shard_map/all_gather | solution.py:79
  63.9 343.8 %reduce-scatter.2.cloned.1.call-start = ((), (), s32[]{:S(2)}) async-start(), calls=%async_computation.4 | async-start | bytes 5242880 | tf_op jit(solution)/shard_map/reduce_scatter | solution.py:287
  208.4 2.3 copy-start.11
  210.9 19.3 %copy-start.1 = (bf16[256,2048]{1,0:T(8,128)(2,1)S(1)}, bf16[256,2048]{1,0:T(8,128)(2,1)}, u32[]{:S(2)}) copy-start(bf16[256,2048]{1,0:T(8,128)(2,1)} %param.18) | copy-start | bytes 3145732
  230.3 6.1 %copy-start.5 = (f32[2048]{0:T(1024)S(1)}, f32[2048]{0:T(1024)}, u32[]{:S(2)}) copy-start(f32[2048]{0:T(1024)} %param.28) | copy-start | bytes 24580
  230.3 46.6 %copy-start.6 = (f32[3,1408]{1,0:T(4,128)S(1)}, f32[3,1408]{1,0:T(4,128)}, u32[]{:S(2)}) copy-start(f32[3,1408]{1,0:T(4,128)} %param.32) | copy-start | bytes 50692
  230.3 46.6 %copy-start.7 = (f32[3,1408]{1,0:T(4,128)S(1)}, f32[3,1408]{1,0:T(4,128)}, u32[]{:S(2)}) copy-start(f32[3,1408]{1,0:T(4,128)} %param.31) | copy-start | bytes 50692
  236.7 18.6 %collective-permute-start = (bf16[256,2048]{1,0:T(8,128)(2,1)S(1)}, bf16[256,2048]{1,0:T(8,128)(2,1)S(1)}, u32[]{:S(2)}, u32[]{:S(2)}) collective-permute-start(bf16[256,2048]{1,0:T(8,128)(2,1)S(1)} %fusion.43), channel_id=1, source_target_pairs={{0,1},{1,2},{2,3},{3,0},{4,5},{5,6},{6,7},{7,4},{8,9},{9,10},{10,1... | collective-permute-start | bytes 3145736 | tf_op jit(solution)/shard_map/ppermute | solution.py:18
  255.3 21.6 %collective-permute-start.1 = (bf16[256,2048]{1,0:T(8,128)(2,1)S(1)}, bf16[256,2048]{1,0:T(8,128)(2,1)S(1)}, u32[]{:S(2)}, u32[]{:S(2)}) collective-permute-start(bf16[256,2048]{1,0:T(8,128)(2,1)S(1)} %collective-permute-done), channel_id=1, source_target_pairs={{0,1},{1,2},{2,3},{3,0},{4,5},{5,6},{6,7},{7,4},{8,9},{9,10},{10,1... | collective-permute-start | bytes 3145736 | tf_op jit(solution)/shard_map/ppermute | solution.py:18
  276.9 21.7 %collective-permute-start.2 = (bf16[256,2048]{1,0:T(8,128)(2,1)S(1)}, bf16[256,2048]{1,0:T(8,128)(2,1)}, u32[]{:S(2)}, u32[]{:S(2)}) collective-permute-start(bf16[256,2048]{1,0:T(8,128)(2,1)S(1)} %collective-permute-done.1), channel_id=1, source_target_pairs={{0,1},{1,2},{2,3},{3,0},{4,5},{5,6},{6,7},{7,4},{8,9},{9,10},{10,1... | collective-permute-start | bytes 3145736 | tf_op jit(solution)/shard_map/ppermute | solution.py:18
  302.2 15.9 %collective-permute-start.3 = (bf16[2,2048]{1,0:T(2,128)(2,1)S(1)}, bf16[2,2048]{1,0:T(2,128)(2,1)S(1)}, u32[]{:S(2)}, u32[]{:S(2)}) collective-permute-start(bf16[2,2048]{1,0:T(2,128)(2,1)S(1)} %constant_dynamic-slice_fusion.3), channel_id=1, source_target_pairs={{0,4},{4,8},{8,12},{12,16},{16,20},{20,24},{24,28},{28,32},{32,36}... | collective-permute-start | bytes 24584 | tf_op jit(solution)/shard_map/ppermute | solution.py:74
  318.1 12.0 %copy-start = (bf16[1024,2048]{1,0:T(8,128)(2,1)S(1)}, bf16[1024,2048]{1,0:T(8,128)(2,1)}, u32[]{:S(2)}) copy-start(bf16[1024,2048]{1,0:T(8,128)(2,1)} %constant_dynamic-slice_fusion.4) | copy-start | bytes 12582916
  318.1 12.0 %copy-start.12 = (bf16[2048,2816]{1,0:T(8,128)(2,1)S(1)}, bf16[2048,2816]{1,0:T(8,128)(2,1)}, u32[]{:S(2)}) copy-start(bf16[2048,2816]{1,0:T(8,128)(2,1)} %all-gather.15.cloned.1.call-done) | copy-start | bytes 34603012
Sparse Core Ops, SparseCore 0:
  9.5 49.5 all-gather.16
  60.8 82.4 all-gather.12
  145.0 20.2 all-gather.18
  167.4 63.4 all-gather.14
  363.1 44.5 reduce-scatter.1
